TPU v7x, 32 devices: a whole 2x2x4 slice. The times are simulated.
32 devices in a mesh: sp: 8 (over z, core), tp: 4 (over y, x).
Axes of the slice: x: 2, y: 2, z: 4, core: 2. Of those that a mesh axis runs over, the one named last changes fastest.
Arguments:
- tokens: bfloat16 [2048, 4096], P('sp'), may hold values from -6 to 6
- norm_gain: float32 [2, 4096], replicated, may hold values from 0.1 to 1.9
- w_outer: bfloat16 [2, 4096, 1024], P(None, 'sp', 'tp'), may hold values from -0.09375 to 0.09375
- w_inner: bfloat16 [2, 4096, 1024], P(None, 'sp', 'tp'), may hold values from -0.09375 to 0.09375
- w_value: bfloat16 [2, 4096, 1024], P(None, 'sp', 'tp'), may hold values from -0.09375 to 0.09375
- w_back: bfloat16 [2, 1024, 4096], P(None, 'sp', 'tp'), may hold values from -0.1875 to 0.1875
- taps: float32 [2, 3, 1024], P(None, None, 'tp'), may hold values from -3 to 3
Outputs:
- result: bfloat16 [2048, 4096], P('sp', 'tp')
All inputs are finite; a program needn't handle non-finite values.
Results may differ from a plain program's by a relative error of at most 0.022.
Values may be sent and summed in bfloat16 or wider, within the bound.
A program may use at most 64 MiB of HBM per device.

v0:
```python
import jax
import jax.numpy as jnp
from jax import lax
from jax.sharding import PartitionSpec as P

eps = 1e-06


def shifted(block, axis, distance):
    devices = range(lax.axis_size(axis))
    route = [(i - distance, i) for i in devices if i - distance in devices]
    return lax.ppermute(block, axis, route)


def per_device(tokens, norm_gain, w_outer, w_inner, w_value, w_back, taps):
    layers = w_outer.shape[0]
    count = tokens.shape[0]
    feats = w_back.shape[2]
    own = lax.axis_index("tp")
    held = (
        lax.all_gather(w_outer, "sp", axis=1, tiled=True),
        lax.all_gather(w_inner, "sp", axis=1, tiled=True),
        lax.all_gather(w_value, "sp", axis=1, tiled=True),
        lax.all_gather(w_back, "sp", axis=1, tiled=True),
    )
    current = tokens
    resid = lax.dynamic_slice_in_dim(tokens, own * feats, feats, 1)
    for layer in range(layers):
        if layer > 0:
            current = lax.all_gather(resid, "tp", axis=1, tiled=True)
        xf = current.astype(jnp.float32)
        normed = (
            xf * lax.rsqrt(jnp.mean(xf * xf, axis=-1, keepdims=True) + eps) * norm_gain[layer]
        ).astype(jnp.bfloat16)
        outer = jnp.dot(normed, held[0][layer], preferred_element_type=jnp.float32)
        inner = jnp.dot(normed, held[1][layer], preferred_element_type=jnp.float32)
        value = jnp.dot(normed, held[2][layer], preferred_element_type=jnp.float32)
        outer = outer.astype(jnp.bfloat16)
        inner = inner.astype(jnp.bfloat16)
        value = value.astype(jnp.bfloat16)
        mixed = (inner.astype(jnp.float32) * value.astype(jnp.float32)).astype(jnp.bfloat16)
        before = shifted(mixed[count - 2 :], "sp", 1)
        padded = jnp.concatenate([before, mixed], axis=0).astype(jnp.float32)
        conv = (
            taps[layer, 0] * padded[:count]
            + taps[layer, 1] * padded[1 : count + 1]
            + taps[layer, 2] * padded[2:]
        )
        gated = (outer.astype(jnp.float32) * conv).astype(jnp.bfloat16)
        whole = lax.all_gather(gated, "tp", axis=1, tiled=True)
        proj = jnp.dot(whole, held[3][layer], preferred_element_type=jnp.float32)
        resid = (resid.astype(jnp.float32) + proj).astype(jnp.bfloat16)
    return resid


def solution(mesh):
    in_specs = (
        P("sp", None),
        P(),
        P(None, "sp", "tp"),
        P(None, "sp", "tp"),
        P(None, "sp", "tp"),
        P(None, "sp", "tp"),
        P(None, None, "tp"),
    )
    out_specs = P("sp", "tp")
    return jax.shard_map(
        per_device, mesh=mesh, in_specs=in_specs, out_specs=out_specs, check_vma=False
    )
```

profile of v0, /device:TPU:1, one launch (start us, length us, event | category | flops | bytes accessed | tf_op | source)
XLA Modules:
  0.0 271.2 jit_solution(8346042315905669766)
XLA Ops:
  6.5 0.0 copy-start
  6.5 0.0 copy-start.3
  6.5 0.0 all-gather.10.cloned.1.call-start
  6.5 0.7 all-gather.10.cloned.1.call-update
  7.3 0.0 all-gather.8.cloned.1.call-start
  7.3 0.7 all-gather.8.cloned.1.call-update
  8.0 0.0 all-gather.6.cloned.1.call-start
  8.1 0.7 all-gather.6.cloned.1.call-update
  8.7 0.0 all-gather.12.cloned.1.call-start
  8.8 0.5 all-gather.12.cloned.1.call-update
  9.3 0.0 all-gather.14.cloned.1.call-start
  9.4 2.1 fusion
  11.5 0.0 copy-done.3
  11.5 46.8 %all-gather.10.cloned.1.call-done = bf16[2,4096,256]{2,1,0:T(8,128)(2,1)} async-done(((bf16[2,512,256]{2,1,0:T(8,128)(2,1)}), bf16[2,4096,256]{2,1,0:T(8,128)(2,1)}) %all-gather.10.cloned.1.call-update) | async-done | bytes 4194320 | tf_op jit(solution)/shard_map/all_gather | solution.py:23
  58.3 0.0 copy-done
  58.3 2.4 fusion.27
  60.7 0.0 copy-start.4
  60.7 44.9 %all-gather.8.cloned.1.call-done = bf16[2,4096,256]{2,1,0:T(8,128)(2,1)} async-done(((bf16[2,512,256]{2,1,0:T(8,128)(2,1)}), bf16[2,4096,256]{2,1,0:T(8,128)(2,1)}) %all-gather.8.cloned.1.call-update) | async-done | bytes 4194320 | tf_op jit(solution)/shard_map/all_gather | solution.py:22
  105.6 2.4 fusion.25
  108.0 2.0 collective-permute-start
  110.0 0.0 copy-done.4
  110.1 1.0 collective-permute-done
  111.1 41.8 %all-gather.6.cloned.1.call-done = bf16[2,4096,256]{2,1,0:T(8,128)(2,1)} async-done(((bf16[2,512,256]{2,1,0:T(8,128)(2,1)}), bf16[2,4096,256]{2,1,0:T(8,128)(2,1)}) %all-gather.6.cloned.1.call-update) | async-done | bytes 4194320 | tf_op jit(solution)/shard_map/all_gather | solution.py:21
  152.9 2.4 fusion.21
  155.3 12.9 %all_gather.24 = bf16[256,1024]{1,0:T(8,128)(2,1)S(1)} all-gather(bf16[256,256]{1,0:T(8,128)(2,1)S(1)} %fusion.21), channel_id=1, replica_groups=mesh['sp'=8,'tp'=4] {'tp'}, dimensions={1}, use_global_device_ids=true | all-gather | bytes 655360 | tf_op jit(solution)/shard_map/all_gather | solution.py:50
  168.2 31.9 %all-gather.12.cloned.1.call-done = bf16[2,1024,1024]{2,1,0:T(8,128)(2,1)} async-done(((bf16[2,128,1024]{2,1,0:T(8,128)(2,1)}), bf16[2,1024,1024]{2,1,0:T(8,128)(2,1)}) %all-gather.12.cloned.1.call-update) | async-done | bytes 4194320 | tf_op jit(solution)/shard_map/all_gather | solution.py:24
  200.1 3.1 %fusion.17 = bf16[256,1024]{1,0:T(8,128)(2,1)} fusion(bf16[256,1024]{1,0:T(8,128)(2,1)S(1)} %all_gather.24, bf16[2,1024,1024]{2,1,0:T(8,128)(2,1)} %all-gather.12.cloned.1.call-done, bf16[256,4096]{1,0:T(8,128)(2,1)S(1)} %copy-done, s32[]{:T(128)S(6)} %select_n.3), kind=kOutput, calls=%fused_computation.29 | convolution fusion | flops 537657344 | bytes 3670020 | tf_op jit(solution)/shard_map/dot_general | solution.py:51
  203.2 0.0 all-gather.14.cloned.1.call-update
  203.2 33.6 %all-gather.14.cloned.1.call-done = bf16[256,4096]{1,0:T(8,128)(2,1)} async-done(((bf16[256,1024]{1,0:T(8,128)(2,1)}), bf16[256,4096]{1,0:T(8,128)(2,1)}) %all-gather.14.cloned.1.call-update) | async-done | bytes 2097168 | tf_op jit(solution)/shard_map/all_gather | solution.py:30
  236.8 2.1 fusion.3
  238.9 0.0 copy-start.1
  238.9 0.0 copy-start.7
  238.9 3.1 %fusion.37 = f32[256,256]{1,0:T(8,128)S(1)} fusion(bf16[2,4096,256]{2,1,0:T(8,128)(2,1)} %all-gather.10.cloned.1.call-done, bf16[256,4096]{1,0:T(8,128)(2,1)} %all-gather.14.cloned.1.call-done, f32[4096]{0:T(1024)S(1)} %bitcast.82, f32[256]{0:T(256)S(1)} %add_rsqrt_fusion), kind=kOutput, calls=%fused_computation.49 | convolution fusion | flops 541196288 | bytes 4473856 | tf_op jit(solution)/shard_map/dot_general | solution.py:37
  242.1 0.0 copy-done.1
  242.1 0.9 copy-done.7
  243.0 0.0 copy-start.6
  243.0 0.8 fusion.35
  243.8 4.0 %collective-permute-start.1 = (bf16[2,256]{1,0:T(2,128)(2,1)S(1)}, bf16[2,256]{1,0:T(2,128)(2,1)S(1)}, u32[]{:S(2)}, u32[]{:S(2)}) collective-permute-start(bf16[2,256]{1,0:T(2,128)(2,1)S(1)} %slice.107), channel_id=1, source_target_pairs={{0,4},{4,8},{8,12},{12,16},{16,20},{20,24},{24,28},{1,5},{5,9},{9,... | collective-permute-start | bytes 3080 | tf_op jit(solution)/shard_map/ppermute | solution.py:12
  247.8 0.7 collective-permute-done.1
  248.5 0.0 copy-done.6
  248.5 0.0 copy-start.2
  248.5 0.0 copy-start.5
  248.5 0.8 fusion.31
  249.3 13.8 %all_gather.27 = bf16[256,1024]{1,0:T(8,128)(2,1)S(1)} all-gather(bf16[256,256]{1,0:T(8,128)(2,1)S(1)} %fusion.31), channel_id=1, replica_groups=mesh['sp'=8,'tp'=4] {'tp'}, dimensions={1}, use_global_device_ids=true | all-gather | bytes 655360 | tf_op jit(solution)/shard_map/all_gather | solution.py:50
  263.2 0.0 copy-done.2
  263.2 0.0 copy-done.5
  263.2 1.5 fusion.16
  (8 shorter events, 0.1 us)
Async XLA Ops:
  6.5 51.8 %copy-start = (bf16[256,4096]{1,0:T(8,128)(2,1)S(1)}, bf16[256,4096]{1,0:T(8,128)(2,1)}, u32[]{:S(2)}) copy-start(bf16[256,4096]{1,0:T(8,128)(2,1)} %param.7) | copy-start | bytes 6291460
  6.5 4.9 %copy-start.3 = (f32[2,4096]{1,0:T(2,128)S(1)}, f32[2,4096]{1,0:T(2,128)}, u32[]{:S(2)}) copy-start(f32[2,4096]{1,0:T(2,128)} %param.8) | copy-start | bytes 98308
  6.5 51.8 %all-gather.10.cloned.1.call-start = ((), (), s32[]{:S(2)}) async-start(), calls=%async_computation.2 | async-start | bytes 4718592 | tf_op jit(solution)/shard_map/all_gather | solution.py:23
  7.3 98.3 %all-gather.8.cloned.1.call-start = ((), (), s32[]{:S(2)}) async-start(), calls=%async_computation.1 | async-start | bytes 4718592 | tf_op jit(solution)/shard_map/all_gather | solution.py:22
  8.0 144.9 %all-gather.6.cloned.1.call-start = ((), (), s32[]{:S(2)}) async-start(), calls=%async_computation | async-start | bytes 4718592 | tf_op jit(solution)/shard_map/all_gather | solution.py:21
  8.7 191.3 %all-gather.12.cloned.1.call-start = ((), (), s32[]{:S(2)}) async-start(), calls=%async_computation.3 | async-start | bytes 4718592 | tf_op jit(solution)/shard_map/all_gather | solution.py:24
  9.3 227.5 %all-gather.14.cloned.1.call-start = ((), (), s32[]{:S(2)}) async-start(), calls=%async_computation.4 | async-start | bytes 2621440 | tf_op jit(solution)/shard_map/all_gather | solution.py:30
  60.7 49.4 %copy-start.4 = (f32[2,3,256]{2,0,1:T(2,128)S(1)}, f32[2,3,256]{2,0,1:T(2,128)}, u32[]{:S(2)}) copy-start(f32[2,3,256]{2,0,1:T(2,128)} %param.13) | copy-start | bytes 18436
  108.0 3.1 %collective-permute-start = (bf16[2,256]{1,0:T(2,128)(2,1)S(1)}, bf16[2,256]{1,0:T(2,128)(2,1)S(1)}, u32[]{:S(2)}, u32[]{:S(2)}) collective-permute-start(bf16[2,256]{1,0:T(2,128)(2,1)S(1)} %slice.99), channel_id=1, source_target_pairs={{0,4},{4,8},{8,12},{12,16},{16,20},{20,24},{24,28},{1,5},{5,9},{9,... | collective-permute-start | bytes 3080 | tf_op jit(solution)/shard_map/ppermute | solution.py:12
  238.9 3.2 %copy-start.1 = (bf16[256,4096]{1,0:T(8,128)(2,1)S(1)}, bf16[256,4096]{1,0:T(8,128)(2,1)}, u32[]{:S(2)}) copy-start(bf16[256,4096]{1,0:T(8,128)(2,1)} %all-gather.14.cloned.1.call-done) | copy-start | bytes 6291460
  238.9 4.1 %copy-start.7 = (bf16[2,4096,256]{2,1,0:T(8,128)(2,1)S(1)}, bf16[2,4096,256]{2,1,0:T(8,128)(2,1)}, u32[]{:S(2)}) copy-start(bf16[2,4096,256]{2,1,0:T(8,128)(2,1)} %all-gather.8.cloned.1.call-done) | copy-start | bytes 12582916
  243.0 5.5 %copy-start.6 = (bf16[2,4096,256]{2,1,0:T(8,128)(2,1)S(1)}, bf16[2,4096,256]{2,1,0:T(8,128)(2,1)}, u32[]{:S(2)}) copy-start(bf16[2,4096,256]{2,1,0:T(8,128)(2,1)} %all-gather.6.cloned.1.call-done) | copy-start | bytes 12582916
  243.8 4.7 %collective-permute-start.1 = (bf16[2,256]{1,0:T(2,128)(2,1)S(1)}, bf16[2,256]{1,0:T(2,128)(2,1)S(1)}, u32[]{:S(2)}, u32[]{:S(2)}) collective-permute-start(bf16[2,256]{1,0:T(2,128)(2,1)S(1)} %slice.107), channel_id=1, source_target_pairs={{0,4},{4,8},{8,12},{12,16},{16,20},{20,24},{24,28},{1,5},{5,9},{9,... | collective-permute-start | bytes 3080 | tf_op jit(solution)/shard_map/ppermute | solution.py:12
  248.5 14.7 %copy-start.2 = (bf16[256,1024]{1,0:T(8,128)(2,1)S(1)}, bf16[256,1024]{1,0:T(8,128)(2,1)}, u32[]{:S(2)}) copy-start(bf16[256,1024]{1,0:T(8,128)(2,1)} %fusion.17) | copy-start | bytes 1572868
  248.5 14.7 %copy-start.5 = (bf16[2,1024,1024]{2,1,0:T(8,128)(2,1)S(1)}, bf16[2,1024,1024]{2,1,0:T(8,128)(2,1)}, u32[]{:S(2)}) copy-start(bf16[2,1024,1024]{2,1,0:T(8,128)(2,1)} %all-gather.12.cloned.1.call-done) | copy-start | bytes 12582916
Sparse Core Ops, SparseCore 0:
  8.9 49.3 all-gather.9
  59.9 45.6 all-gather.7
  107.2 45.6 all-gather.5
  154.4 45.6 all-gather.11
  203.4 33.4 all-gather.13
where the time goes:
time: 272 us; the launch traced here: 271 us
  waiting for transfers between devices  203 us (75%)
  blocking collectives  26.8 us (10%)
  matrix products  16.4 us (6%)
  between operations  13.3 us (5%)
  starting transfers between devices  6.16 us (2%)
  other arithmetic  4.24 us (2%)
    all_gather x1, waiting for transfers between devices, per_device(): lax.all_gather(w_value, 'sp', axis=1, tiled=True)  46.8 us
    all_gather x1, waiting for transfers between devices, per_device(): lax.all_gather(w_inner, 'sp', axis=1, tiled=True)  44.9 us
    all_gather x1, waiting for transfers between devices, per_device(): lax.all_gather(w_outer, 'sp', axis=1, tiled=True)  41.8 us
    all_gather x1, waiting for transfers between devices, per_device(): current = lax.all_gather(resid, 'tp', axis=1, tiled=True)  33.6 us
    all_gather x1, waiting for transfers between devices, per_device(): lax.all_gather(w_back, 'sp', axis=1, tiled=True)  31.9 us
    all_gather x2, blocking collectives, per_device(): whole = lax.all_gather(gated, 'tp', axis=1, tiled=True)  26.8 us
    ppermute x2, starting transfers between devices, shifted(): return lax.ppermute(block, axis, route)  6.01 us
    dot_general x2, matrix products, per_device(): value = jnp.dot(normed, held[2][layer], preferred_element_type=jnp.float32)  5.49 us
  transfers between devices with their start and end apart: 7, of which 7 were waited for; matrix products, arithmetic and copies ran while one was open for 3% of the time, Pallas kernels for 0%

commit v1 on v0

--- a/solution.py
+++ b/solution.py
@@ -1,7 +1,15 @@
+import functools
+
 import jax
 import jax.numpy as jnp
 from jax import lax
+from jax.experimental import pallas as pl
+from jax.experimental.pallas import tpu as pltpu
 from jax.sharding import PartitionSpec as P
+
+MESH = pl.DeviceIdType.MESH
+f32 = jnp.float32
+bf16 = jnp.bfloat16
 
 eps = 1e-06
 
@@ -53,6 +61,377 @@
     return resid
 
 
+def mixer_kernel(
+    tok, gain, w_outer, w_inner, w_value, w_back, taps, out,
+    xs, win, wback, acc, ss, gat, mixed, halo, res, landed,
+    sem_local, sem_tok_local, tok_send, tok_recv, w_send, w_recv,
+    g_send, g_recv, h_send, h_recv, o_send, o_recv,
+):
+    s, t = lax.axis_index("sp"), lax.axis_index("tp")
+    n_sp, n_tp = win.shape[1], xs.shape[1]
+    layers = wback.shape[0]
+    rows = tok.shape[0]
+    feats = xs.shape[3]
+    units = 4 * layers
+    core = lax.rem(s, 2)
+    flip = 1 - 2 * core
+    left = s < n_sp // 2
+    side = jnp.where(left, 1, -1)
+    plane = lax.div(s, 2)
+    is_end = jnp.logical_or(plane == 0, plane == n_sp // 2 - 1)
+    is_mid = jnp.logical_not(is_end)
+    partner = s + flip
+    inward = jnp.where(is_end, s + 2 * side, s)
+    end = jnp.where(is_mid, s - 2 * side, s)
+    opp = jnp.where(is_mid, s + 2 * side, s)
+    oppend = jnp.where(is_mid, s + 4 * side, s)
+    tx = t + 1 - 2 * lax.rem(t, 2)
+    ty = t + 2 - 4 * lax.div(t, 2)
+    td = n_tp - 1 - t
+
+    barrier = pltpu.get_barrier_semaphore()
+    for k in range(1, n_sp):
+        pl.semaphore_signal(barrier, inc=1, device_id=(lax.rem(s + k, n_sp), t), device_id_type=MESH)
+    for other in (tx, ty):
+        pl.semaphore_signal(barrier, inc=1, device_id=(s, other), device_id_type=MESH)
+    pl.semaphore_wait(barrier, n_sp + 1)
+
+    projections = (w_outer, w_inner, w_value)
+
+    def own_w(u):
+        layer, m = u // 4, u % 4
+        return projections[m].at[layer] if m < 3 else w_back.at[layer]
+
+    def held_w(u, source):
+        layer, m = u // 4, u % 4
+        return win.at[3 * layer + m, source] if m < 3 else wback.at[layer, source]
+
+    def remote(a, b, ssem, rsem, sp, tp):
+        return pltpu.make_async_remote_copy(
+            src_ref=a, dst_ref=b, send_sem=ssem, recv_sem=rsem, device_id=(sp, tp), device_id_type=MESH
+        )
+
+    def send_w(u, source, kind, target, own=False):
+        a = own_w(u) if own else held_w(u, source)
+        remote(a, held_w(u, source), w_send.at[u, kind], w_recv.at[u, source], target, t).start()
+
+    def wait_w(u, source):
+        remote(held_w(u, source), held_w(u, source), w_send.at[u, 0], w_recv.at[u, source], partner, t).wait_recv()
+
+    def tok_cols(j):
+        return tok.at[:, pl.ds(pl.multiple_of(j * feats, feats), feats)]
+
+    def tok_to_end_mid():
+        target = lax.div(s, 2) + 2
+        place = xs.at[0, t, pl.ds(pl.multiple_of(core * rows, rows), rows)]
+        return remote(tok_cols(t), place, tok_send.at[0], tok_recv.at[core], target, t)
+
+    outer_mid = jnp.logical_or(s == 2, s == n_sp - 3)
+    my_half = pl.multiple_of(jnp.where(left, 1, 0) * rows, rows)
+    partner_half = pl.multiple_of(jnp.where(left, 0, 1) * rows, rows)
+
+    def tok_local(j):
+        return pltpu.make_async_copy(tok_cols(j), xs.at[0, j, pl.ds(my_half, rows)], sem_tok_local.at[j])
+
+    def tok_partner(j):
+        return remote(tok_cols(j), xs.at[0, j, pl.ds(partner_half, rows)], tok_send.at[j], tok_recv.at[j], partner, t)
+
+    def result_copy(b):
+        return remote(res.at[b], landed, o_send.at[b], o_recv, 2 * (s - 2) + b, t)
+
+    def result_wait():
+        remote(landed, landed, o_send.at[0], o_recv, partner, t).wait_recv()
+        out[...] = landed[...]
+
+    @pl.when(is_end)
+    def _():
+        sends = []
+        for u in range(units):
+            send_w(u, s, 0, inward, own=True)
+            if u == 0:
+                tok_to_end_mid().start()
+        for u in range(units):
+            remote(own_w(u), held_w(u, s), w_send.at[u, 0], w_recv.at[u, s], inward, t).wait_send()
+        tok_to_end_mid().wait_send()
+        result_wait()
+
+    def gather_pieces(g, buf):
+        size = buf.shape[1] // 2
+        def piece(block, half, k, target):
+            ref = buf.at[block, pl.ds(half * size, size)]
+            return remote(ref, ref, g_send.at[g, k], g_recv.at[g, k], s, target)
+        return piece
+
+    def gather_start(g, buf):
+        p = gather_pieces(g, buf)
+        p(t, 0, 0, tx).start()
+        p(t, 1, 1, ty).start()
+        p(t, 1, 2, tx).start()
+        p(t, 0, 3, ty).start()
+
+    def gather_forward(g, buf):
+        p = gather_pieces(g, buf)
+        p(tx, 0, 0, tx).wait_recv()
+        p(tx, 0, 4, ty).start()
+        p(ty, 1, 1, ty).wait_recv()
+        p(ty, 1, 5, tx).start()
+
+    def gather_near(g, buf):
+        p = gather_pieces(g, buf)
+        p(tx, 1, 2, tx).wait_recv()
+        p(ty, 0, 3, ty).wait_recv()
+
+    def gather_far(g, buf):
+        p = gather_pieces(g, buf)
+        p(td, 0, 4, ty).wait_recv()
+        p(td, 1, 5, tx).wait_recv()
+
+    def gather_drain(g, buf):
+        p = gather_pieces(g, buf)
+        p(t, 0, 0, tx).wait_send()
+        p(t, 1, 1, ty).wait_send()
+        p(t, 1, 2, tx).wait_send()
+        p(t, 0, 3, ty).wait_send()
+        p(tx, 0, 4, ty).wait_send()
+        p(ty, 1, 5, tx).wait_send()
+
+    def take_end(u):
+        wait_w(u, end)
+        send_w(u, end, 2, opp)
+        send_w(u, end, 3, partner)
+
+    def pump(u):
+        if u + 1 < units:
+            take_end(u + 1)
+        if u + 4 < units:
+            send_w(u + 4, s, 0, opp, own=True)
+        wait_w(u, opp)
+        send_w(u, opp, 4, partner)
+        wait_w(u, oppend)
+        send_w(u, oppend, 5, partner)
+
+    def settle(u):
+        pltpu.make_async_copy(own_w(u), held_w(u, s), sem_local.at[u]).wait()
+        for source in (s, end, opp, oppend):
+            wait_w(u, source + flip)
+
+    def project(layer, j, first):
+        def tile(r, carry):
+            span = pl.ds(pl.multiple_of(r * rows, rows), rows)
+            x = xs[layer, j, span, :].astype(f32)
+            sq = x * x
+            part = sq[:, :128]
+            for q in range(1, feats // 128):
+                part = part + sq[:, 128 * q : 128 * (q + 1)]
+            scaled = (x * gain[layer, pl.ds(j, 1), :]).astype(bf16)
+            depth = win.shape[2]
+            per = feats // depth
+            dots = []
+            for m in range(3):
+                w = win[3 * layer + m, pl.ds(per * j, per)].reshape(feats, win.shape[3])
+                dots.append(jnp.dot(scaled, w, preferred_element_type=f32))
+            if first:
+                ss[span, :] = part
+                for m in range(3):
+                    acc[m, span, :] = dots[m]
+            else:
+                ss[span, :] += part
+                for m in range(3):
+                    acc[m, span, :] += dots[m]
+            return carry
+        lax.fori_loop(0, 2, tile, 0)
+
+    def halo_copy(layer):
+        count = 2 * rows
+        return remote(
+            mixed.at[pl.ds(count - 16, 16)], halo.at[layer], h_send.at[layer], h_recv.at[layer], s + 1, t
+        )
+
+    def gate(layer):
+        width = feats * n_tp
+        inv = lax.rsqrt(jnp.sum(ss[...], axis=-1, keepdims=True) / width + eps)
+        inner = (acc[1] * inv).astype(bf16)
+        value = (acc[2] * inv).astype(bf16)
+        mix = (inner.astype(f32) * value.astype(f32)).astype(bf16)
+        if layer > 0:
+            @pl.when(s < n_sp - 3)
+            def _():
+                halo_copy(layer - 1).wait_send()
+        mixed[...] = mix
+        @pl.when(s < n_sp - 3)
+        def _():
+            halo_copy(layer).start()
+        outer = (acc[0] * inv).astype(bf16).astype(f32)
+        @pl.when(s == 2)
+        def _():
+            halo[layer] = jnp.zeros(halo.shape[1:], bf16)
+        @pl.when(s > 2)
+        def _():
+            halo_copy(layer).wait_recv()
+        now = mix.astype(f32)
+        tail = halo[layer].astype(f32)
+        row = lax.broadcasted_iota(jnp.int32, now.shape, 0)
+        one = jnp.where(row == 0, tail[15:16], pltpu.roll(now, 1, 0))
+        two = pltpu.roll(now, 2, 0)
+        two = jnp.where(row == 0, tail[14:15], jnp.where(row == 1, tail[15:16], two))
+        conv = taps[layer, 0:1] * two + taps[layer, 1:2] * one + taps[layer, 2:3] * now
+        gat[layer, t] = (outer * conv).astype(bf16)
+
+    def back(layer, b):
+        span = pl.ds(b * rows, rows)
+        total = xs[layer, t, span, :].astype(f32)
+        depth = gat.shape[3]
+        per = depth // wback.shape[2]
+        for j in range(n_tp):
+            w = wback[layer, per * j : per * (j + 1)].reshape(depth, feats)
+            total = total + jnp.dot(gat[layer, j, span, :], w, preferred_element_type=f32)
+        return total.astype(bf16)
+
+    @pl.when(is_mid)
+    def _():
+        for u in range(min(4, units)):
+            send_w(u, s, 0, opp, own=True)
+        for u in range(units):
+            pltpu.make_async_copy(own_w(u), held_w(u, s), sem_local.at[u]).start()
+        @pl.when(outer_mid)
+        def _():
+            for j in range(n_tp):
+                tok_partner(j).start()
+        @pl.when(jnp.logical_not(outer_mid))
+        def _():
+            for j in range(n_tp):
+                tok_local(j).start()
+        for u in range(units):
+            send_w(u, s, 1, partner, own=True)
+        take_end(0)
+        pump(0)
+        first = xs.at[0]
+        @pl.when(outer_mid)
+        def _():
+            for b in range(2):
+                place = xs.at[0, t, pl.ds(b * rows, rows)]
+                remote(place, place, tok_send.at[b], tok_recv.at[b], partner, t).wait_recv()
+            gather_start(0, first)
+        pump(1)
+        @pl.when(outer_mid)
+        def _():
+            gather_forward(0, first)
+        pump(2)
+        @pl.when(outer_mid)
+        def _():
+            gather_near(0, first)
+            gather_far(0, first)
+        @pl.when(jnp.logical_not(outer_mid))
+        def _():
+            for j in range(n_tp):
+                tok_local(j).wait()
+                tok_partner(j).wait_recv()
+        for layer in range(layers):
+            for m in range(3):
+                settle(4 * layer + m)
+            x_g, gate_g = 2 * layer, 2 * layer + 1
+            if layer == 0:
+                for k, j in enumerate((t, tx, ty, td)):
+                    project(layer, j, k == 0)
+            else:
+                project(layer, t, True)
+                gather_near(x_g, xs.at[layer])
+                project(layer, tx, False)
+                project(layer, ty, False)
+                gather_far(x_g, xs.at[layer])
+                project(layer, td, False)
+            gate(layer)
+            gather_start(gate_g, gat.at[layer])
+            pump(4 * layer + 3)
+            gather_forward(gate_g, gat.at[layer])
+            settle(4 * layer + 3)
+            gather_near(gate_g, gat.at[layer])
+            gather_far(gate_g, gat.at[layer])
+            if layer + 1 < layers:
+                for b in range(2):
+                    xs[layer + 1, t, b * rows : (b + 1) * rows, :] = back(layer, b)
+                gather_start(x_g + 2, xs.at[layer + 1])
+                pump(4 * layer + 4)
+                gather_forward(x_g + 2, xs.at[layer + 1])
+                pump(4 * layer + 5)
+                pump(4 * layer + 6)
+            else:
+                for b in range(2):
+                    mine = s == (n_sp // 2 - b)
+                    res[b] = back(layer, b)
+                    @pl.when(mine)
+                    def _():
+                        out[...] = res[b]
+                    @pl.when(jnp.logical_not(mine))
+                    def _():
+                        result_copy(b).start()
+        for u in range(units):
+            for kind in range(6):
+                remote(own_w(u), held_w(u, s), w_send.at[u, kind], w_recv.at[u, s], partner, t).wait_send()
+        for layer in range(layers):
+            if layer > 0:
+                gather_drain(2 * layer, xs.at[layer])
+            gather_drain(2 * layer + 1, gat.at[layer])
+        @pl.when(outer_mid)
+        def _():
+            gather_drain(0, first)
+            for j in range(n_tp):
+                tok_partner(j).wait_send()
+        @pl.when(s < n_sp - 3)
+        def _():
+            halo_copy(layers - 1).wait_send()
+        for b in range(2):
+            @pl.when(s != (n_sp // 2 - b))
+            def _():
+                result_copy(b).wait_send()
+        @pl.when(outer_mid)
+        def _():
+            result_wait()
+
+
+def fused(tokens, norm_gain, w_outer, w_inner, w_value, w_back, taps):
+    n_sp, n_tp = lax.axis_size("sp"), lax.axis_size("tp")
+    rows, width = tokens.shape
+    layers, depth, chans = w_outer.shape
+    back_rows, feats = w_back.shape[1:]
+    dma = pltpu.SemaphoreType.DMA
+    hbm, vmem = pl.BlockSpec(memory_space=pl.ANY), pl.BlockSpec(memory_space=pltpu.VMEM)
+    return pl.pallas_call(
+        mixer_kernel,
+        out_shape=jax.ShapeDtypeStruct((rows, feats), bf16),
+        in_specs=[hbm, vmem, hbm, hbm, hbm, hbm, vmem],
+        out_specs=vmem,
+        scratch_shapes=[
+            pltpu.VMEM((layers, n_tp, 2 * rows, feats), bf16),
+            pltpu.VMEM((3 * layers, n_sp, depth, chans), bf16),
+            pltpu.VMEM((layers, n_sp, back_rows, feats), bf16),
+            pltpu.VMEM((3, 2 * rows, chans), f32),
+            pltpu.VMEM((2 * rows, 128), f32),
+            pltpu.VMEM((layers, n_tp, 2 * rows, chans), bf16),
+            pltpu.VMEM((2 * rows, chans), bf16),
+            pltpu.VMEM((layers, 16, chans), bf16),
+            pltpu.VMEM((2, rows, feats), bf16),
+            pltpu.VMEM((rows, feats), bf16),
+            dma((4 * layers,)),
+            dma((n_tp,)),
+            dma((n_tp,)),
+            dma((n_tp,)),
+            dma((4 * layers, 6)),
+            dma((4 * layers, n_sp)),
+            dma((2 * layers, 6)),
+            dma((2 * layers, 6)),
+            dma((layers,)),
+            dma((layers,)),
+            dma((2,)),
+            dma,
+        ],
+        compiler_params=pltpu.CompilerParams(
+            collective_id=0, has_side_effects=True, vmem_limit_bytes=60 * 1024 * 1024
+        ),
+        name="mixer",
+    )(tokens, norm_gain.reshape(layers, n_tp, feats), w_outer, w_inner, w_value, w_back, taps)
+
+
 def solution(mesh):
     in_specs = (
         P("sp", None),
@@ -64,6 +443,7 @@
         P(None, None, "tp"),
     )
     out_specs = P("sp", "tp")
+    body = fused if (mesh.shape["sp"], mesh.shape["tp"]) == (8, 4) else per_device
     return jax.shard_map(
-        per_device, mesh=mesh, in_specs=in_specs, out_specs=out_specs, check_vma=False
+        body, mesh=mesh, in_specs=in_specs, out_specs=out_specs, check_vma=False
     )

time: 272 us -> 143 us (0.53)
  waiting for transfers between devices: 203 us -> 0 us
  Pallas kernels: 0 us -> 138 us
  blocking collectives: 26.8 us -> 0 us
  matrix products: 16.4 us -> 0 us
  between operations: 13.3 us -> 0.01 us
  starting transfers between devices: 6.16 us -> 0 us
  other arithmetic: 4.24 us -> 0 us
  local copies, waits for them, and re-layouts: 0.98 us -> 4.56 us
    all_gather x5 -> x0, waiting for transfers between devices: 199 us -> none  [the longest x1 46.8 us: per_device(): lax.all_gather(w_value, 'sp', axis=1, tiled=True)]
    pallas_call x0 -> x1, Pallas kernels: none -> 138 us  [fused(): pl.pallas_call(mixer_kernel, out_shape=jax.ShapeDtypeStruct((rows, feats)...]
    all_gather x2 -> x0, blocking collectives: 26.8 us -> none  [per_device(): whole = lax.all_gather(gated, 'tp', axis=1, tiled=True)]
    dot_general x8 -> x0, matrix products: 16.4 us -> none  [the longest x2 5.49 us: per_device(): value = jnp.dot(normed, held[2][layer], preferred_element_type=jnp.float32)]
    ppermute x2 -> x0, starting transfers between devices: 6.01 us -> none  [shifted(): return lax.ppermute(block, axis, route)]
    reduce_sum x2 -> x0, other arithmetic: 4.17 us -> none  [per_device(): jnp.mean(xf * xf, axis=-1, keepdims=True) + eps]
  transfers between devices with their start and end apart: 7 -> 0, of which waited for: 7 -> 0; matrix products, arithmetic and copies ran while one was open for 3% -> 0% of each run, Pallas kernels for 0% -> 0%
where the time goes in v1:
time: 143 us; the launch traced here: 142 us
  Pallas kernels  138 us (97%)
  local copies, waits for them, and re-layouts  4.56 us (3%)
    pallas_call x1, Pallas kernels, fused(): pl.pallas_call(mixer_kernel, out_shape=jax.ShapeDtypeStruct((rows, feats)...  138 us
    unnamed x2, local copies, waits for them, and re-layouts  3.15 us

profile of v1, /device:TPU:1, one launch (start us, length us, event | category | flops | bytes accessed | tf_op | source)
XLA Modules:
  0.0 142.5 jit_solution(6298578654431468806)
XLA Ops:
  0.0 1.3 copy.8.taps
  1.3 1.4 reshape.3.gain
  2.7 137.9 %mixer.1 = bf16[256,1024]{1,0:T(8,128)(2,1)} custom-call(bf16[256,4096]{1,0:T(8,128)(2,1)} %tok.1, f32[2,4,1024]{2,1,0:T(4,128)} %reshape.3.gain, bf16[2,512,256]{2,1,0:T(8,128)(2,1)} %w_outer.1, bf16[2,512,256]{2,1,0:T(8,128)(2,1)} %w_inner.1, bf16[2,512,256]{2,1,0:T(8,128)(2,1)} %w_value.1, bf16[2,128,1024]{2,1,0:T(8,128)(2,1)} %w_back.1, ...), custom_call_target="tpu_custom_call" | custom-call | tf_op jit(solution)/shard_map/mixer/pallas_call | solution.py:399
  140.6 1.9 %copy.10 = bf16[256,1024]{1,0:T(8,128)(2,1)} copy(bf16[256,1024]{1,0:T(8,128)(2,1)} %mixer.1) | data formatting | bytes 1048576

commit v2 on v1

--- a/solution.py
+++ b/solution.py
@@ -63,16 +63,18 @@
 
 def mixer_kernel(
     tok, gain, w_outer, w_inner, w_value, w_back, taps, out,
-    xs, win, wback, acc, ss, gat, mixed, halo, res, landed,
+    xs, x_last, win, wback, acc, ss, gat, gat_last, mixed, mixed_last, halo, res,
     sem_local, sem_tok_local, tok_send, tok_recv, w_send, w_recv,
     g_send, g_recv, h_send, h_recv, o_send, o_recv,
 ):
     s, t = lax.axis_index("sp"), lax.axis_index("tp")
-    n_sp, n_tp = win.shape[1], xs.shape[1]
+    n_sp, n_tp = win.shape[1], x_last.shape[0]
     layers = wback.shape[0]
     rows = tok.shape[0]
-    feats = xs.shape[3]
+    feats = x_last.shape[2]
     units = 4 * layers
+    last = layers - 1
+    spread = 4 * last
     core = lax.rem(s, 2)
     flip = 1 - 2 * core
     left = s < n_sp // 2
@@ -137,23 +139,8 @@
         return remote(tok_cols(j), xs.at[0, j, pl.ds(partner_half, rows)], tok_send.at[j], tok_recv.at[j], partner, t)
 
     def result_copy(b):
-        return remote(res.at[b], landed, o_send.at[b], o_recv, 2 * (s - 2) + b, t)
-
-    def result_wait():
-        remote(landed, landed, o_send.at[0], o_recv, partner, t).wait_recv()
-        out[...] = landed[...]
-
-    @pl.when(is_end)
-    def _():
-        sends = []
-        for u in range(units):
-            send_w(u, s, 0, inward, own=True)
-            if u == 0:
-                tok_to_end_mid().start()
-        for u in range(units):
-            remote(own_w(u), held_w(u, s), w_send.at[u, 0], w_recv.at[u, s], inward, t).wait_send()
-        tok_to_end_mid().wait_send()
-        result_wait()
+        return remote(res.at[b], x_last.at[t], o_send.at[b], o_recv, 2 * (s - 2) + b, t)
+
 
     def gather_pieces(g, buf):
         size = buf.shape[1] // 2
@@ -206,24 +193,42 @@
         if u + 4 < units:
             send_w(u + 4, s, 0, opp, own=True)
         wait_w(u, opp)
+        if u >= spread:
+            send_w(u, opp, 7, end)
         send_w(u, opp, 4, partner)
         wait_w(u, oppend)
+        if u >= spread:
+            send_w(u, oppend, 8, end)
         send_w(u, oppend, 5, partner)
+
+    def end_feed(u):
+        for k in (1, 2, 3):
+            source = s + 2 * k * side
+            wait_w(u, source)
+            send_w(u, source, 2 + k, partner)
+
+    def feed(u):
+        @pl.when(is_mid)
+        def _():
+            pump(u)
+        @pl.when(is_end)
+        def _():
+            end_feed(u)
 
     def settle(u):
         pltpu.make_async_copy(own_w(u), held_w(u, s), sem_local.at[u]).wait()
-        for source in (s, end, opp, oppend):
-            wait_w(u, source + flip)
-
-    def project(layer, j, first):
+        for source in range(0, n_sp, 2):
+            wait_w(u, source + 1 - core)
+
+    def project(layer, x_ref, j, first):
         def tile(r, carry):
             span = pl.ds(pl.multiple_of(r * rows, rows), rows)
-            x = xs[layer, j, span, :].astype(f32)
+            x = x_ref[j, span, :].astype(f32)
             sq = x * x
             part = sq[:, :128]
             for q in range(1, feats // 128):
                 part = part + sq[:, 128 * q : 128 * (q + 1)]
-            scaled = (x * gain[layer, pl.ds(j, 1), :]).astype(bf16)
+            scaled = (x * gain[layer : layer + 1, pl.ds(pl.multiple_of(j * feats, feats), feats)]).astype(bf16)
             depth = win.shape[2]
             per = feats // depth
             dots = []
@@ -239,35 +244,32 @@
                 for m in range(3):
                     acc[m, span, :] += dots[m]
             return carry
-        lax.fori_loop(0, 2, tile, 0)
-
-    def halo_copy(layer):
-        count = 2 * rows
+        lax.fori_loop(0, x_ref.shape[1] // rows, tile, 0)
+
+    def halo_copy(layer, mix_ref):
+        count = mix_ref.shape[0]
         return remote(
-            mixed.at[pl.ds(count - 16, 16)], halo.at[layer], h_send.at[layer], h_recv.at[layer], s + 1, t
+            mix_ref.at[pl.ds(count - 16, 16)], halo.at[layer], h_send.at[layer], h_recv.at[layer], s + 1, t
         )
 
-    def gate(layer):
+    def gate(layer, mix_ref, gat_ref, begin, final):
         width = feats * n_tp
-        inv = lax.rsqrt(jnp.sum(ss[...], axis=-1, keepdims=True) / width + eps)
-        inner = (acc[1] * inv).astype(bf16)
-        value = (acc[2] * inv).astype(bf16)
+        span = pl.ds(0, mix_ref.shape[0])
+        inv = lax.rsqrt(jnp.sum(ss[span, :], axis=-1, keepdims=True) / width + eps)
+        inner = (acc[1, span, :] * inv).astype(bf16)
+        value = (acc[2, span, :] * inv).astype(bf16)
         mix = (inner.astype(f32) * value.astype(f32)).astype(bf16)
-        if layer > 0:
-            @pl.when(s < n_sp - 3)
-            def _():
-                halo_copy(layer - 1).wait_send()
-        mixed[...] = mix
-        @pl.when(s < n_sp - 3)
-        def _():
-            halo_copy(layer).start()
-        outer = (acc[0] * inv).astype(bf16).astype(f32)
-        @pl.when(s == 2)
+        mix_ref[...] = mix
+        @pl.when(s < final)
+        def _():
+            halo_copy(layer, mix_ref).start()
+        outer = (acc[0, span, :] * inv).astype(bf16).astype(f32)
+        @pl.when(s == begin)
         def _():
             halo[layer] = jnp.zeros(halo.shape[1:], bf16)
-        @pl.when(s > 2)
-        def _():
-            halo_copy(layer).wait_recv()
+        @pl.when(s > begin)
+        def _():
+            halo_copy(layer, mix_ref).wait_recv()
         now = mix.astype(f32)
         tail = halo[layer].astype(f32)
         row = lax.broadcasted_iota(jnp.int32, now.shape, 0)
@@ -275,24 +277,41 @@
         two = pltpu.roll(now, 2, 0)
         two = jnp.where(row == 0, tail[14:15], jnp.where(row == 1, tail[15:16], two))
         conv = taps[layer, 0:1] * two + taps[layer, 1:2] * one + taps[layer, 2:3] * now
-        gat[layer, t] = (outer * conv).astype(bf16)
-
-    def back(layer, b):
+        gat_ref[t] = (outer * conv).astype(bf16)
+
+    def back(layer, x_ref, gat_ref, b):
         span = pl.ds(b * rows, rows)
-        total = xs[layer, t, span, :].astype(f32)
-        depth = gat.shape[3]
+        total = x_ref[t, span, :].astype(f32)
+        depth = gat_ref.shape[2]
         per = depth // wback.shape[2]
         for j in range(n_tp):
             w = wback[layer, per * j : per * (j + 1)].reshape(depth, feats)
-            total = total + jnp.dot(gat[layer, j, span, :], w, preferred_element_type=f32)
+            total = total + jnp.dot(gat_ref[j, span, :], w, preferred_element_type=f32)
         return total.astype(bf16)
+
+    def mine(b):
+        return s == n_sp // 2 - b
+
+    for u in range(units):
+        @pl.when(jnp.logical_or(is_mid, u >= spread))
+        def _():
+            pltpu.make_async_copy(own_w(u), held_w(u, s), sem_local.at[u]).start()
+
+    @pl.when(is_end)
+    def _():
+        for u in range(units):
+            send_w(u, s, 0, inward, own=True)
+            if u == 0:
+                tok_to_end_mid().start()
+        for u in range(spread, units):
+            send_w(u, s, 1, partner, own=True)
 
     @pl.when(is_mid)
     def _():
         for u in range(min(4, units)):
             send_w(u, s, 0, opp, own=True)
-        for u in range(units):
-            pltpu.make_async_copy(own_w(u), held_w(u, s), sem_local.at[u]).start()
+        for u in range(spread, units):
+            send_w(u, s, 6, end, own=True)
         @pl.when(outer_mid)
         def _():
             for j in range(n_tp):
@@ -326,67 +345,101 @@
             for j in range(n_tp):
                 tok_local(j).wait()
                 tok_partner(j).wait_recv()
-        for layer in range(layers):
+        for layer in range(last):
+            x_ref, gat_ref = xs.at[layer], gat.at[layer]
+            if layer > 0:
+                for m in range(3):
+                    pump(4 * layer + m)
+                gather_forward(2 * layer, x_ref)
+                gather_near(2 * layer, x_ref)
+                gather_far(2 * layer, x_ref)
             for m in range(3):
                 settle(4 * layer + m)
-            x_g, gate_g = 2 * layer, 2 * layer + 1
-            if layer == 0:
-                for k, j in enumerate((t, tx, ty, td)):
-                    project(layer, j, k == 0)
-            else:
-                project(layer, t, True)
-                gather_near(x_g, xs.at[layer])
-                project(layer, tx, False)
-                project(layer, ty, False)
-                gather_far(x_g, xs.at[layer])
-                project(layer, td, False)
-            gate(layer)
-            gather_start(gate_g, gat.at[layer])
+            for k, j in enumerate((t, tx, ty, td)):
+                project(layer, x_ref, j, k == 0)
+            gate(layer, mixed.at[layer], gat_ref, 2, n_sp - 3)
+            gather_start(2 * layer + 1, gat_ref)
             pump(4 * layer + 3)
-            gather_forward(gate_g, gat.at[layer])
+            gather_forward(2 * layer + 1, gat_ref)
             settle(4 * layer + 3)
-            gather_near(gate_g, gat.at[layer])
-            gather_far(gate_g, gat.at[layer])
-            if layer + 1 < layers:
-                for b in range(2):
-                    xs[layer + 1, t, b * rows : (b + 1) * rows, :] = back(layer, b)
-                gather_start(x_g + 2, xs.at[layer + 1])
-                pump(4 * layer + 4)
-                gather_forward(x_g + 2, xs.at[layer + 1])
-                pump(4 * layer + 5)
-                pump(4 * layer + 6)
-            else:
-                for b in range(2):
-                    mine = s == (n_sp // 2 - b)
-                    res[b] = back(layer, b)
-                    @pl.when(mine)
+            gather_near(2 * layer + 1, gat_ref)
+            gather_far(2 * layer + 1, gat_ref)
+            for b in range(2):
+                if layer + 1 < last:
+                    xs[layer + 1, t, b * rows : (b + 1) * rows, :] = back(layer, x_ref, gat_ref, b)
+                else:
+                    res[b] = back(layer, x_ref, gat_ref, b)
+                    @pl.when(mine(b))
                     def _():
-                        out[...] = res[b]
-                    @pl.when(jnp.logical_not(mine))
+                        x_last[t] = res[b]
+                    @pl.when(jnp.logical_not(mine(b)))
                     def _():
                         result_copy(b).start()
+            if layer + 1 < last:
+                gather_start(2 * layer + 2, xs.at[layer + 1])
+
+    @pl.when(jnp.logical_not(jnp.logical_or(mine(0), mine(1))))
+    def _():
+        remote(res.at[0], x_last.at[t], o_send.at[0], o_recv, partner, t).wait_recv()
+    gather_start(2 * last, x_last)
+    feed(spread)
+    gather_forward(2 * last, x_last)
+    feed(spread + 1)
+    feed(spread + 2)
+    for m in range(3):
+        settle(spread + m)
+    project(last, x_last, t, True)
+    gather_near(2 * last, x_last)
+    project(last, x_last, tx, False)
+    project(last, x_last, ty, False)
+    gather_far(2 * last, x_last)
+    project(last, x_last, td, False)
+    gate(last, mixed_last, gat_last, 0, n_sp - 1)
+    gather_start(2 * last + 1, gat_last)
+    feed(spread + 3)
+    gather_forward(2 * last + 1, gat_last)
+    settle(spread + 3)
+    gather_near(2 * last + 1, gat_last)
+    gather_far(2 * last + 1, gat_last)
+    out[...] = back(last, x_last, gat_last, 0)
+
+    def sent_w(u, kind):
+        remote(own_w(u), held_w(u, s), w_send.at[u, kind], w_recv.at[u, s], partner, t).wait_send()
+
+    @pl.when(is_end)
+    def _():
         for u in range(units):
-            for kind in range(6):
-                remote(own_w(u), held_w(u, s), w_send.at[u, kind], w_recv.at[u, s], partner, t).wait_send()
-        for layer in range(layers):
+            for kind in (0, 1, 3, 4, 5) if u >= spread else (0,):
+                sent_w(u, kind)
+        tok_to_end_mid().wait_send()
+
+    @pl.when(is_mid)
+    def _():
+        for u in range(units):
+            for kind in range(9 if u >= spread else 6):
+                sent_w(u, kind)
+        for layer in range(last):
             if layer > 0:
                 gather_drain(2 * layer, xs.at[layer])
             gather_drain(2 * layer + 1, gat.at[layer])
+            @pl.when(s < n_sp - 3)
+            def _():
+                halo_copy(layer, mixed.at[layer]).wait_send()
         @pl.when(outer_mid)
         def _():
-            gather_drain(0, first)
+            gather_drain(0, xs.at[0])
             for j in range(n_tp):
                 tok_partner(j).wait_send()
-        @pl.when(s < n_sp - 3)
-        def _():
-            halo_copy(layers - 1).wait_send()
         for b in range(2):
-            @pl.when(s != (n_sp // 2 - b))
+            @pl.when(jnp.logical_not(mine(b)))
             def _():
                 result_copy(b).wait_send()
-        @pl.when(outer_mid)
-        def _():
-            result_wait()
+
+    gather_drain(2 * last, x_last)
+    gather_drain(2 * last + 1, gat_last)
+    @pl.when(s < n_sp - 1)
+    def _():
+        halo_copy(last, mixed_last).wait_send()
 
 
 def fused(tokens, norm_gain, w_outer, w_inner, w_value, w_back, taps):
@@ -402,21 +455,23 @@
         in_specs=[hbm, vmem, hbm, hbm, hbm, hbm, vmem],
         out_specs=vmem,
         scratch_shapes=[
-            pltpu.VMEM((layers, n_tp, 2 * rows, feats), bf16),
+            pltpu.VMEM((layers - 1, n_tp, 2 * rows, feats), bf16),
+            pltpu.VMEM((n_tp, rows, feats), bf16),
             pltpu.VMEM((3 * layers, n_sp, depth, chans), bf16),
             pltpu.VMEM((layers, n_sp, back_rows, feats), bf16),
             pltpu.VMEM((3, 2 * rows, chans), f32),
             pltpu.VMEM((2 * rows, 128), f32),
-            pltpu.VMEM((layers, n_tp, 2 * rows, chans), bf16),
-            pltpu.VMEM((2 * rows, chans), bf16),
+            pltpu.VMEM((layers - 1, n_tp, 2 * rows, chans), bf16),
+            pltpu.VMEM((n_tp, rows, chans), bf16),
+            pltpu.VMEM((layers - 1, 2 * rows, chans), bf16),
+            pltpu.VMEM((rows, chans), bf16),
             pltpu.VMEM((layers, 16, chans), bf16),
             pltpu.VMEM((2, rows, feats), bf16),
-            pltpu.VMEM((rows, feats), bf16),
             dma((4 * layers,)),
             dma((n_tp,)),
             dma((n_tp,)),
             dma((n_tp,)),
-            dma((4 * layers, 6)),
+            dma((4 * layers, 9)),
             dma((4 * layers, n_sp)),
             dma((2 * layers, 6)),
             dma((2 * layers, 6)),
@@ -429,7 +484,7 @@
             collective_id=0, has_side_effects=True, vmem_limit_bytes=60 * 1024 * 1024
         ),
         name="mixer",
-    )(tokens, norm_gain.reshape(layers, n_tp, feats), w_outer, w_inner, w_value, w_back, taps)
+    )(tokens, norm_gain, w_outer, w_inner, w_value, w_back, taps)
 
 
 def solution(mesh):

time: 143 us -> 151 us (1.056); the launches traced: 142 us -> 148 us
  Pallas kernels: 138 us -> 145 us
    pallas_call x1, Pallas kernels: 138 us -> 145 us  [fused(): pl.pallas_call(mixer_kernel, out_shape=jax.ShapeDtypeStruct((rows, feats)...]
where the time goes in v2:
time: 151 us; the launch traced here: 148 us
  Pallas kernels  145 us (96%)
  local copies, waits for them, and re-layouts  3.16 us (2%)
    pallas_call x1, Pallas kernels, fused(): pl.pallas_call(mixer_kernel, out_shape=jax.ShapeDtypeStruct((rows, feats)...  145 us
    unnamed x2, local copies, waits for them, and re-layouts  3.16 us

profile of v2, /device:TPU:1, one launch (start us, length us, event | category | flops | bytes accessed | tf_op | source)
XLA Modules:
  0.0 148.4 jit_solution(5032810309255187496)
XLA Ops:
  0.0 1.3 copy.8.taps
  1.3 145.2 %mixer.1 = bf16[256,1024]{1,0:T(8,128)(2,1)} custom-call(bf16[256,4096]{1,0:T(8,128)(2,1)} %tok.1, f32[2,4096]{1,0:T(2,128)} %gain.1, bf16[2,512,256]{2,1,0:T(8,128)(2,1)} %w_outer.1, bf16[2,512,256]{2,1,0:T(8,128)(2,1)} %w_inner.1, bf16[2,512,256]{2,1,0:T(8,128)(2,1)} %w_value.1, bf16[2,128,1024]{2,1,0:T(8,128)(2,1)} %w_back.1, f32[2,3,256]{2,1,0:T(4,128)} %copy.8.taps), custom_call_target="tpu_custom_call" | custom-call | tf_op jit(solution)/shard_map/mixer/pallas_call | solution.py:452
  146.5 1.9 %copy.10 = bf16[256,1024]{1,0:T(8,128)(2,1)} copy(bf16[256,1024]{1,0:T(8,128)(2,1)} %mixer.1) | data formatting | bytes 1048576

commit v3 on v1

--- a/solution.py
+++ b/solution.py
@@ -223,7 +223,7 @@
             part = sq[:, :128]
             for q in range(1, feats // 128):
                 part = part + sq[:, 128 * q : 128 * (q + 1)]
-            scaled = (x * gain[layer, pl.ds(j, 1), :]).astype(bf16)
+            scaled = (x * gain[layer : layer + 1, pl.ds(pl.multiple_of(j * feats, feats), feats)]).astype(bf16)
             depth = win.shape[2]
             per = feats // depth
             dots = []
@@ -274,7 +274,7 @@
         one = jnp.where(row == 0, tail[15:16], pltpu.roll(now, 1, 0))
         two = pltpu.roll(now, 2, 0)
         two = jnp.where(row == 0, tail[14:15], jnp.where(row == 1, tail[15:16], two))
-        conv = taps[layer, 0:1] * two + taps[layer, 1:2] * one + taps[layer, 2:3] * now
+        conv = taps[0, layer : layer + 1] * two + taps[1, layer : layer + 1] * one + taps[2, layer : layer + 1] * now
         gat[layer, t] = (outer * conv).astype(bf16)
 
     def back(layer, b):
@@ -304,7 +304,6 @@
         for u in range(units):
             send_w(u, s, 1, partner, own=True)
         take_end(0)
-        pump(0)
         first = xs.at[0]
         @pl.when(outer_mid)
         def _():
@@ -312,10 +311,11 @@
                 place = xs.at[0, t, pl.ds(b * rows, rows)]
                 remote(place, place, tok_send.at[b], tok_recv.at[b], partner, t).wait_recv()
             gather_start(0, first)
+        pump(0)
+        @pl.when(outer_mid)
+        def _():
+            gather_forward(0, first)
         pump(1)
-        @pl.when(outer_mid)
-        def _():
-            gather_forward(0, first)
         pump(2)
         @pl.when(outer_mid)
         def _():
@@ -341,14 +341,29 @@
                 gather_far(x_g, xs.at[layer])
                 project(layer, td, False)
             gate(layer)
-            gather_start(gate_g, gat.at[layer])
+            g = gather_pieces(gate_g, gat.at[layer])
+            g(t, 0, 0, tx).start()
+            g(t, 0, 3, ty).start()
+            g(t, 1, 1, ty).start()
+            g(t, 1, 2, tx).start()
             pump(4 * layer + 3)
-            gather_forward(gate_g, gat.at[layer])
+            g(tx, 0, 0, tx).wait_recv()
+            g(tx, 0, 4, ty).start()
+            g(ty, 1, 1, ty).wait_recv()
+            g(ty, 1, 5, tx).start()
             settle(4 * layer + 3)
-            gather_near(gate_g, gat.at[layer])
-            gather_far(gate_g, gat.at[layer])
+
+            def take_gated(b):
+                if b == 0:
+                    g(ty, 0, 3, ty).wait_recv()
+                    g(td, 0, 4, ty).wait_recv()
+                else:
+                    g(tx, 1, 2, tx).wait_recv()
+                    g(td, 1, 5, tx).wait_recv()
+
             if layer + 1 < layers:
                 for b in range(2):
+                    take_gated(b)
                     xs[layer + 1, t, b * rows : (b + 1) * rows, :] = back(layer, b)
                 gather_start(x_g + 2, xs.at[layer + 1])
                 pump(4 * layer + 4)
@@ -358,6 +373,7 @@
             else:
                 for b in range(2):
                     mine = s == (n_sp // 2 - b)
+                    take_gated(b)
                     res[b] = back(layer, b)
                     @pl.when(mine)
                     def _():
@@ -429,7 +445,7 @@
             collective_id=0, has_side_effects=True, vmem_limit_bytes=60 * 1024 * 1024
         ),
         name="mixer",
-    )(tokens, norm_gain.reshape(layers, n_tp, feats), w_outer, w_inner, w_value, w_back, taps)
+    )(tokens, norm_gain, w_outer, w_inner, w_value, w_back, taps.transpose(1, 0, 2))
 
 
 def solution(mesh):

time: 143 us -> 139 us (0.972)
  local copies, waits for them, and re-layouts: 4.56 us -> 1.87 us
  Pallas kernels: 138 us -> 136 us
    pallas_call x1, Pallas kernels: 138 us -> 136 us  [fused(): pl.pallas_call(mixer_kernel, out_shape=jax.ShapeDtypeStruct((rows, feats)...]
    unnamed x2 -> x1, local copies, waits for them, and re-layouts: 3.15 us -> 1.87 us
where the time goes in v3:
time: 139 us; the launch traced here: 138 us
  Pallas kernels  136 us (98%)
  local copies, waits for them, and re-layouts  1.87 us (1%)
    pallas_call x1, Pallas kernels, fused(): pl.pallas_call(mixer_kernel, out_shape=jax.ShapeDtypeStruct((rows, feats)...  136 us

profile of v3, /device:TPU:1, one launch (start us, length us, event | category | flops | bytes accessed | tf_op | source)
XLA Modules:
  0.0 138.2 jit_solution(8441976147457087312)
XLA Ops:
  0.0 136.3 %mixer.1 = bf16[256,1024]{1,0:T(8,128)(2,1)} custom-call(bf16[256,4096]{1,0:T(8,128)(2,1)} %tok.1, f32[2,4096]{1,0:T(2,128)} %gain.1, bf16[2,512,256]{2,1,0:T(8,128)(2,1)} %w_outer.1, bf16[2,512,256]{2,1,0:T(8,128)(2,1)} %w_inner.1, bf16[2,512,256]{2,1,0:T(8,128)(2,1)} %w_value.1, bf16[2,128,1024]{2,1,0:T(8,128)(2,1)} %w_back.1, f32[3,2,256]{2,1,0:T(2,128)} %bitcast.1), custom_call_target="tpu_custom_call" | custom-call | tf_op jit(solution)/shard_map/mixer/pallas_call | solution.py:415
  136.3 1.9 %copy.9 = bf16[256,1024]{1,0:T(8,128)(2,1)} copy(bf16[256,1024]{1,0:T(8,128)(2,1)} %mixer.1) | data formatting | bytes 1048576
